TPU v7x, 32 devices: a whole 2x2x4 slice. The times are simulated.
32 devices in a mesh: grp: 2 (over x), ep: 8 (over z, y), tp: 2 (over core).
Axes of the slice: x: 2, y: 2, z: 4, core: 2. Of those that a mesh axis runs over, the one named last changes fastest.
Arguments:
- tokens: bfloat16 [3072, 2048], P(('grp', 'ep'), 'tp'), parts along dimension 0, may hold values from -10 to 10
- gain_in: float32 [2048], replicated, may hold values from 0.1 to 1.9
- gain_out: float32 [2048], replicated, may hold values from 0.1 to 1.9
- expert_ids: int32 [3072, 2], P(('grp', 'ep')), parts along dimension 0, may hold values from 0 to 3, all different within a row; in each aligned block of 192 rows (0 to 191, 192 to 383, ...) at most 144 rows name the same one
- route_weight: float32 [3072, 2], P(('grp', 'ep')), parts along dimension 0, may hold values from 0.1 to 1
- gate_weight: bfloat16 [8, 2048, 1792], P('ep', None, 'tp'), may hold values from -0.125 to 0.125
- up_weight: bfloat16 [8, 2048, 1792], P('ep', None, 'tp'), may hold values from -0.125 to 0.125
- down_weight: bfloat16 [8, 1792, 2048], P('ep', 'tp'), may hold values from -1 to 1
Outputs:
- layer_out: bfloat16 [3072, 2048], P(('grp', 'ep'), 'tp'), parts along dimension 0
There are 2 independent parts, one for each index of `grp`. A program takes and returns all parts, laid end to end along the dimension named above; an argument that names none is the same for every part. Nothing has to cross between parts.
Inputs may be any that keep to these rules, and one draw needn't show every extreme that they name: `expert_ids`: each row names 2 different experts. Among the tokens of one index of ep no expert is named more than 144 times, a bound that some block reaches.
All inputs are finite; a program needn't handle non-finite values.
Results may differ from a plain program's by a relative error of at most 0.0077.
Values may be sent and summed in bfloat16 or wider, within the bound.
No kernel may reach another device: no remote copies, remote signals or barrier semaphores. Data moves between devices by JAX's collectives and lax.ppermute only.
A program may use at most 64 MiB of HBM per device.

v0:
```python
import jax
import jax.numpy as jnp
from jax import lax
from jax.sharding import PartitionSpec as P

norm_eps = 1e-06


def shards(
    tokens, gain_in, gain_out, expert_ids, route_weight, gate_weight, up_weight, down_weight
):
    bf16, f32 = jnp.bfloat16, jnp.float32
    tok_rows, half_width = tokens.shape
    full_width = 2 * half_width
    ep_size = lax.axis_size("ep")
    expert_count = ep_size // 2
    picks = expert_ids.shape[1]
    capacity = tok_rows * picks * 3 // (2 * expert_count)
    pair = lax.axis_index("ep") // 2
    core = lax.axis_index("tp")
    own_cols = core * half_width
    other_cols = (1 - core) * half_width

    def swap_core(value):
        return lax.ppermute(value, "tp", [(0, 1), (1, 0)])

    def swap_half(value):
        return lax.ppermute(value, "ep", [(i, i ^ 1) for i in range(ep_size)])

    def shift_pair(value, step):
        return lax.ppermute(value, "ep", [(i, (i + 2 * step) % ep_size) for i in range(ep_size)])

    flat_ids = expert_ids.reshape(-1)
    onehot = (flat_ids[:, None] == jnp.arange(expert_count, dtype=jnp.int32)[None, :]).astype(
        jnp.int32
    )
    before = jnp.cumsum(onehot, axis=0) - onehot
    slots = jnp.sum(before * onehot, axis=1).reshape(tok_rows, picks)
    away = (expert_ids - pair + expert_count) % expert_count
    targets = away * capacity + slots

    own_float = tokens.astype(f32)
    squares = lax.psum(jnp.sum(own_float * own_float, axis=1), "tp")
    factor = lax.rsqrt(squares / full_width + norm_eps)[:, None]
    own_gain = lax.dynamic_slice_in_dim(gain_in, own_cols, half_width)
    normed = (own_float * factor * own_gain).astype(bf16)

    steps = [0]
    for near in range(1, expert_count // 2 + 1):
        steps += [near] if 2 * near == expert_count else [near, expert_count - near]

    def pack(step):
        rows = jnp.arange(capacity, dtype=jnp.int32)[:, None] + step * capacity
        placing = jnp.zeros((capacity, tok_rows), bf16)
        for which in range(picks):
            placing = placing + (rows == targets[None, :, which]).astype(bf16)
        return jnp.dot(placing, normed, preferred_element_type=f32).astype(bf16)

    sent = [pack(step) for step in steps]
    mine = [sent[0]]
    for k, step in enumerate(steps[1:], 1):
        mine.append(shift_pair(sent[k], step))
    theirs = []
    for k in range(expert_count):
        theirs.append(swap_half(mine[k]))

    gate_own = lax.dynamic_slice_in_dim(gate_weight[0], own_cols, half_width, 0)
    gate_other = lax.dynamic_slice_in_dim(gate_weight[0], other_cols, half_width, 0)
    up_own = lax.dynamic_slice_in_dim(up_weight[0], own_cols, half_width, 0)
    up_other = lax.dynamic_slice_in_dim(up_weight[0], other_cols, half_width, 0)
    down_own = lax.dynamic_slice_in_dim(down_weight[0], own_cols, half_width, 1)
    down_other = lax.dynamic_slice_in_dim(down_weight[0], other_cols, half_width, 1)

    half_sums = []
    for k in range(expert_count):
        here = jnp.concatenate([mine[k], theirs[k]], axis=0)
        there = jnp.concatenate([swap_core(mine[k]), swap_core(theirs[k])], axis=0)
        gate_pre = jnp.dot(here, gate_own, preferred_element_type=f32) + jnp.dot(
            there, gate_other, preferred_element_type=f32
        )
        up_pre = jnp.dot(here, up_own, preferred_element_type=f32) + jnp.dot(
            there, up_other, preferred_element_type=f32
        )
        hidden = (jax.nn.silu(gate_pre) * up_pre).astype(bf16)
        if k > 1:
            hidden, half_sums[k - 1] = lax.optimization_barrier((hidden, half_sums[k - 1]))
        part_other = jnp.dot(hidden, down_other, preferred_element_type=f32).astype(bf16)
        swapped = swap_core(part_other)
        part_own = jnp.dot(hidden, down_own, preferred_element_type=f32).astype(bf16)
        half_sums.append((part_own.astype(f32) + swapped.astype(f32)).astype(bf16))
    if expert_count > 1:
        half_sums[0], half_sums[-1] = lax.optimization_barrier((half_sums[0], half_sums[-1]))
    returned = []
    for k, step in enumerate(steps):
        crossed = swap_half(half_sums[k][capacity:])
        whole = (half_sums[k][:capacity].astype(f32) + crossed.astype(f32)).astype(bf16)
        returned.append(whole if step == 0 else shift_pair(whole, -step))

    high = lax.reduce_precision(route_weight, 8, 7)
    low = (route_weight - high).astype(bf16)
    high = high.astype(bf16)
    routed = jnp.zeros((tok_rows, half_width), f32)
    for k, step in enumerate(steps):
        cols = jnp.arange(capacity, dtype=jnp.int32)[None, :] + step * capacity
        for weight in (high, low):
            mixing = jnp.zeros((tok_rows, capacity), bf16)
            for which in range(picks):
                mixing = mixing + jnp.where(
                    cols == targets[:, which][:, None], weight[:, which][:, None], jnp.zeros((), bf16)
                )
            routed = routed + jnp.dot(mixing, returned[k], preferred_element_type=f32)
    squares_out = lax.psum(jnp.sum(routed * routed, axis=1), "tp")
    factor_out = lax.rsqrt(squares_out / full_width + norm_eps)[:, None]
    own_gain_out = lax.dynamic_slice_in_dim(gain_out, own_cols, half_width)
    return (routed * factor_out * own_gain_out).astype(bf16)


def solution(mesh):
    in_specs = (
        P(("grp", "ep"), "tp"),
        P(),
        P(),
        P(("grp", "ep"), None),
        P(("grp", "ep"), None),
        P("ep", None, "tp"),
        P("ep", None, "tp"),
        P("ep", "tp", None),
    )
    out_specs = P(("grp", "ep"), "tp")
    return jax.shard_map(shards, mesh=mesh, in_specs=in_specs, out_specs=out_specs, check_vma=False)
```

profile of v0, /device:TPU:0, one launch (start us, length us, event | category | flops | bytes accessed | tf_op | source)
XLA Modules:
  0.0 121.1 jit_solution(14318429057756444543)
XLA Ops:
  1.2 1.2 %reduce-window.6 = s32[4,3,128]{2,1,0:T(4,128)S(1)} reduce-window(s32[4,3,128]{2,1,0:T(4,128)S(1)} %fusion.238, s32[]{:T(128)} %constant.65.clone.1), window={size=1x1x128 pad=0_0x0_0x127_0}, to_apply=%region_0.1 | reduce-window | flops 195072 | bytes 12292 | tf_op jit(solution)/shard_map/reduce-window
  3.8 1.2 fusion.138
  5.0 2.6 %psum.14 = f32[192]{0:T(256)S(1)} all-reduce(f32[192]{0:T(256)S(1)} %fusion.138), channel_id=1, replica_groups=mesh['grp'=2,'ep'=8,'tp'=2] {'tp'}, use_global_device_ids=true, to_apply=%region_4.5 | all-reduce | flops 192 | bytes 1536 | tf_op jit(solution)/shard_map/psum | solution.py:43
  8.3 1.3 %convolution_convert_fusion.3 = bf16[144,1024]{1,0:T(8,128)(2,1)S(1)} fusion(s32[192]{0:T(256)S(1)} %bitcast.171, s32[192]{0:T(256)S(1)} %bitcast.159, bf16[192,1024]{1,0:T(8,128)(2,1)} %param.8, f32[1024]{0:T(1024)S(1)} %dynamic_slice.36, f32[192]{0:T(256)S(1)} %add_rsqrt_fusion.1), kind=kOutput, calls=%fused_computation.78 | convolution fusion | flops 57778176 | bytes 694528 | tf_op jit(solution)/shard_map/dot_general | solution.py:57
  9.7 2.9 %collective-permute-start = (bf16[144,1024]{1,0:T(8,128)(2,1)S(1)}, bf16[144,1024]{1,0:T(8,128)(2,1)S(1)}, u32[]{:S(2)}, u32[]{:S(2)}) collective-permute-start(bf16[144,1024]{1,0:T(8,128)(2,1)S(1)} %convolution_convert_fusion.3), channel_id=1, source_target_pairs={{0,2},{2,0},{4,6},{6,4},{8,10},{10,8},{12,14},{14,12},{1,3},{3,1},... | collective-permute-start | bytes 884744 | tf_op jit(solution)/shard_map/ppermute | solution.py:28
  12.9 2.7 %collective-permute-start.4 = (bf16[144,1024]{1,0:T(8,128)(2,1)S(1)}, bf16[144,1024]{1,0:T(8,128)(2,1)S(1)}, u32[]{:S(2)}, u32[]{:S(2)}) collective-permute-start(bf16[144,1024]{1,0:T(8,128)(2,1)S(1)} %convolution_convert_fusion.2), channel_id=1, source_target_pairs={{0,8},{2,10},{4,12},{6,14},{8,0},{10,2},{12,4},{14,6},{1,9},{3,11}... | collective-permute-start | bytes 884744 | tf_op jit(solution)/shard_map/ppermute | solution.py:31
  16.0 1.4 %collective-permute-start.8 = (bf16[144,1024]{1,0:T(8,128)(2,1)S(1)}, bf16[144,1024]{1,0:T(8,128)(2,1)S(1)}, u32[]{:S(2)}, u32[]{:S(2)}) collective-permute-start(bf16[144,1024]{1,0:T(8,128)(2,1)S(1)} %convolution_convert_fusion.1), channel_id=1, source_target_pairs={{0,12},{2,14},{4,0},{6,2},{8,4},{10,6},{12,8},{14,10},{1,13},{3,15... | collective-permute-start | bytes 884744 | tf_op jit(solution)/shard_map/ppermute | solution.py:31
  17.7 0.9 collective-permute-start.12
  18.7 11.5 %collective-permute-done.4 = bf16[144,1024]{1,0:T(8,128)(2,1)S(1)} collective-permute-done((bf16[144,1024]{1,0:T(8,128)(2,1)S(1)}, bf16[144,1024]{1,0:T(8,128)(2,1)S(1)}, u32[]{:S(2)}, u32[]{:S(2)}) %collective-permute-start.4) | collective-permute-done | bytes 294944 | tf_op jit(solution)/shard_map/ppermute | solution.py:31
  30.5 1.9 %collective-permute-start.9 = (bf16[144,1024]{1,0:T(8,128)(2,1)S(1)}, bf16[144,1024]{1,0:T(8,128)(2,1)S(1)}, u32[]{:S(2)}, u32[]{:S(2)}) collective-permute-start(bf16[144,1024]{1,0:T(8,128)(2,1)S(1)} %collective-permute-done.8), channel_id=1, source_target_pairs={{0,2},{2,0},{4,6},{6,4},{8,10},{10,8},{12,14},{14,12},{1,3},{3,1},... | collective-permute-start | bytes 884744 | tf_op jit(solution)/shard_map/ppermute | solution.py:28
  32.7 4.4 %collective-permute-done.12 = bf16[144,1024]{1,0:T(8,128)(2,1)S(1)} collective-permute-done((bf16[144,1024]{1,0:T(8,128)(2,1)S(1)}, bf16[144,1024]{1,0:T(8,128)(2,1)S(1)}, u32[]{:S(2)}, u32[]{:S(2)}) %collective-permute-start.12) | collective-permute-done | bytes 294944 | tf_op jit(solution)/shard_map/ppermute | solution.py:31
  37.2 2.4 %fusion.46 = f32[288,896]{1,0:T(8,128)S(1)} fusion(bf16[1,2048,896]{2,1,0:T(8,128)(2,1)} %param.13, s32[]{:T(128)} %select_n.76, bf16[144,1024]{1,0:T(8,128)(2,1)S(1)} %collective-permute-done, bf16[144,1024]{1,0:T(8,128)(2,1)S(1)} %convolution_convert_fusion.3), kind=kOutput, calls=%fused_computation.46 | convolution fusion | flops 529661952 | bytes 3457536 | tf_op jit(solution)/shard_map/dot_general | solution.py:78
  43.4 1.2 copy-done.4
  50.0 1.0 collective-permute-done.13
  53.4 0.9 multiply_convert_fusion
  61.8 7.9 %collective-permute-done.20 = bf16[144,1024]{1,0:T(8,128)(2,1)S(1)} collective-permute-done((bf16[144,1024]{1,0:T(8,128)(2,1)S(1)}, bf16[144,1024]{1,0:T(8,128)(2,1)S(1)}, u32[]{:S(2)}, u32[]{:S(2)}) %collective-permute-start.20) | collective-permute-done | bytes 294944 | tf_op jit(solution)/shard_map/ppermute | solution.py:28
  69.7 10.3 %collective-permute-start.21 = (bf16[144,1024]{1,0:T(8,128)(2,1)S(1)}, bf16[144,1024]{1,0:T(8,128)(2,1)S(1)}, u32[]{:S(2)}, u32[]{:S(2)}) collective-permute-start(bf16[144,1024]{1,0:T(8,128)(2,1)S(1)} %add_convert_fusion.6), channel_id=1, source_target_pairs={{0,12},{2,14},{4,0},{6,2},{8,4},{10,6},{12,8},{14,10},{1,13},{3,15... | collective-permute-start | bytes 884744 | tf_op jit(solution)/shard_map/ppermute | solution.py:31
  83.0 3.0 %collective-permute-done.21 = bf16[144,1024]{1,0:T(8,128)(2,1)S(1)} collective-permute-done((bf16[144,1024]{1,0:T(8,128)(2,1)S(1)}, bf16[144,1024]{1,0:T(8,128)(2,1)S(1)}, u32[]{:S(2)}, u32[]{:S(2)}) %collective-permute-start.21) | collective-permute-done | bytes 294944 | tf_op jit(solution)/shard_map/ppermute | solution.py:31
  86.4 4.7 %collective-permute-done.22 = bf16[144,1024]{1,0:T(8,128)(2,1)S(1)} collective-permute-done((bf16[144,1024]{1,0:T(8,128)(2,1)S(1)}, bf16[144,1024]{1,0:T(8,128)(2,1)S(1)}, u32[]{:S(2)}, u32[]{:S(2)}) %collective-permute-start.22) | collective-permute-done | bytes 294944 | tf_op jit(solution)/shard_map/ppermute | solution.py:28
  93.0 8.6 %collective-permute-done.23 = bf16[144,1024]{1,0:T(8,128)(2,1)S(1)} collective-permute-done((bf16[144,1024]{1,0:T(8,128)(2,1)S(1)}, bf16[144,1024]{1,0:T(8,128)(2,1)S(1)}, u32[]{:S(2)}, u32[]{:S(2)}) %collective-permute-start.23) | collective-permute-done | bytes 294944 | tf_op jit(solution)/shard_map/ppermute | solution.py:31
  103.1 6.7 %collective-permute-done.19 = bf16[144,1024]{1,0:T(8,128)(2,1)S(1)} collective-permute-done((bf16[144,1024]{1,0:T(8,128)(2,1)S(1)}, bf16[144,1024]{1,0:T(8,128)(2,1)S(1)}, u32[]{:S(2)}, u32[]{:S(2)}) %collective-permute-start.19) | collective-permute-done | bytes 294944 | tf_op jit(solution)/shard_map/ppermute | solution.py:28
  110.1 6.3 %collective-permute-done.25 = bf16[144,1024]{1,0:T(8,128)(2,1)S(1)} collective-permute-done((bf16[144,1024]{1,0:T(8,128)(2,1)S(1)}, bf16[144,1024]{1,0:T(8,128)(2,1)S(1)}, u32[]{:S(2)}, u32[]{:S(2)}) %collective-permute-start.25) | collective-permute-done | bytes 294944 | tf_op jit(solution)/shard_map/ppermute | solution.py:31
  117.7 2.5 %psum.15 = f32[192]{0:T(256)S(1)} all-reduce(f32[192]{0:T(256)S(1)} %get-tuple-element.25), channel_id=1, replica_groups=mesh['grp'=2,'ep'=8,'tp'=2] {'tp'}, use_global_device_ids=true, to_apply=%region_6.7 | all-reduce | flops 192 | bytes 1536 | tf_op jit(solution)/shard_map/psum | solution.py:112
  120.2 0.9 multiply_convert_fusion.4
  (122 shorter events, 32.3 us)
Async XLA Ops:
  9.7 22.7 %collective-permute-start = (bf16[144,1024]{1,0:T(8,128)(2,1)S(1)}, bf16[144,1024]{1,0:T(8,128)(2,1)S(1)}, u32[]{:S(2)}, u32[]{:S(2)}) collective-permute-start(bf16[144,1024]{1,0:T(8,128)(2,1)S(1)} %convolution_convert_fusion.3), channel_id=1, source_target_pairs={{0,2},{2,0},{4,6},{6,4},{8,10},{10,8},{12,14},{14,12},{1,3},{3,1},... | collective-permute-start | bytes 884744 | tf_op jit(solution)/shard_map/ppermute | solution.py:28
  12.6 17.9 %collective-permute-start.1 = (bf16[144,1024]{1,0:T(8,128)(2,1)S(1)}, bf16[144,1024]{1,0:T(8,128)(2,1)S(1)}, u32[]{:S(2)}, u32[]{:S(2)}) collective-permute-start(bf16[144,1024]{1,0:T(8,128)(2,1)S(1)} %convolution_convert_fusion.3), channel_id=1, source_target_pairs={{0,1},{1,0},{2,3},{3,2},{4,5},{5,4},{6,7},{7,6},{8,9},{9,8},{10,11... | collective-permute-start | bytes 884744 | tf_op jit(solution)/shard_map/ppermute | solution.py:25
  12.9 17.2 %collective-permute-start.4 = (bf16[144,1024]{1,0:T(8,128)(2,1)S(1)}, bf16[144,1024]{1,0:T(8,128)(2,1)S(1)}, u32[]{:S(2)}, u32[]{:S(2)}) collective-permute-start(bf16[144,1024]{1,0:T(8,128)(2,1)S(1)} %convolution_convert_fusion.2), channel_id=1, source_target_pairs={{0,8},{2,10},{4,12},{6,14},{8,0},{10,2},{12,4},{14,6},{1,9},{3,11}... | collective-permute-start | bytes 884744 | tf_op jit(solution)/shard_map/ppermute | solution.py:31
  16.0 14.5 %collective-permute-start.8 = (bf16[144,1024]{1,0:T(8,128)(2,1)S(1)}, bf16[144,1024]{1,0:T(8,128)(2,1)S(1)}, u32[]{:S(2)}, u32[]{:S(2)}) collective-permute-start(bf16[144,1024]{1,0:T(8,128)(2,1)S(1)} %convolution_convert_fusion.1), channel_id=1, source_target_pairs={{0,12},{2,14},{4,0},{6,2},{8,4},{10,6},{12,8},{14,10},{1,13},{3,15... | collective-permute-start | bytes 884744 | tf_op jit(solution)/shard_map/ppermute | solution.py:31
  17.7 19.4 %collective-permute-start.12 = (bf16[144,1024]{1,0:T(8,128)(2,1)S(1)}, bf16[144,1024]{1,0:T(8,128)(2,1)S(1)}, u32[]{:S(2)}, u32[]{:S(2)}) collective-permute-start(bf16[144,1024]{1,0:T(8,128)(2,1)S(1)} %convolution_convert_fusion), channel_id=1, source_target_pairs={{0,4},{2,6},{4,8},{6,10},{8,12},{10,14},{12,0},{14,2},{1,5},{3,7},... | collective-permute-start | bytes 884744 | tf_op jit(solution)/shard_map/ppermute | solution.py:31
  30.2 15.2 %collective-permute-start.5 = (bf16[144,1024]{1,0:T(8,128)(2,1)S(1)}, bf16[144,1024]{1,0:T(8,128)(2,1)S(1)}, u32[]{:S(2)}, u32[]{:S(2)}) collective-permute-start(bf16[144,1024]{1,0:T(8,128)(2,1)S(1)} %collective-permute-done.4), channel_id=1, source_target_pairs={{0,2},{2,0},{4,6},{6,4},{8,10},{10,8},{12,14},{14,12},{1,3},{3,1},... | collective-permute-start | bytes 884744 | tf_op jit(solution)/shard_map/ppermute | solution.py:28
  30.5 16.3 %collective-permute-start.6 = (bf16[144,1024]{1,0:T(8,128)(2,1)S(1)}, bf16[144,1024]{1,0:T(8,128)(2,1)S(1)}, u32[]{:S(2)}, u32[]{:S(2)}) collective-permute-start(bf16[144,1024]{1,0:T(8,128)(2,1)S(1)} %collective-permute-done.4), channel_id=1, source_target_pairs={{0,1},{1,0},{2,3},{3,2},{4,5},{5,4},{6,7},{7,6},{8,9},{9,8},{10,11... | collective-permute-start | bytes 884744 | tf_op jit(solution)/shard_map/ppermute | solution.py:25
  30.5 17.2 %collective-permute-start.9 = (bf16[144,1024]{1,0:T(8,128)(2,1)S(1)}, bf16[144,1024]{1,0:T(8,128)(2,1)S(1)}, u32[]{:S(2)}, u32[]{:S(2)}) collective-permute-start(bf16[144,1024]{1,0:T(8,128)(2,1)S(1)} %collective-permute-done.8), channel_id=1, source_target_pairs={{0,2},{2,0},{4,6},{6,4},{8,10},{10,8},{12,14},{14,12},{1,3},{3,1},... | collective-permute-start | bytes 884744 | tf_op jit(solution)/shard_map/ppermute | solution.py:28
  32.4 16.7 %collective-permute-start.10 = (bf16[144,1024]{1,0:T(8,128)(2,1)S(1)}, bf16[144,1024]{1,0:T(8,128)(2,1)S(1)}, u32[]{:S(2)}, u32[]{:S(2)}) collective-permute-start(bf16[144,1024]{1,0:T(8,128)(2,1)S(1)} %collective-permute-done.8), channel_id=1, source_target_pairs={{0,1},{1,0},{2,3},{3,2},{4,5},{5,4},{6,7},{7,6},{8,9},{9,8},{10,11... | collective-permute-start | bytes 884744 | tf_op jit(solution)/shard_map/ppermute | solution.py:25
  37.1 3.4 %collective-permute-start.2 = (bf16[144,1024]{1,0:T(8,128)(2,1)S(1)}, bf16[144,1024]{1,0:T(8,128)(2,1)S(1)}, u32[]{:S(2)}, u32[]{:S(2)}) collective-permute-start(bf16[144,1024]{1,0:T(8,128)(2,1)S(1)} %collective-permute-done), channel_id=1, source_target_pairs={{0,1},{1,0},{2,3},{3,2},{4,5},{5,4},{6,7},{7,6},{8,9},{9,8},{10,11... | collective-permute-start | bytes 884744 | tf_op jit(solution)/shard_map/ppermute | solution.py:25
  40.5 10.4 %collective-permute-start.13 = (bf16[144,1024]{1,0:T(8,128)(2,1)S(1)}, bf16[144,1024]{1,0:T(8,128)(2,1)S(1)}, u32[]{:S(2)}, u32[]{:S(2)}) collective-permute-start(bf16[144,1024]{1,0:T(8,128)(2,1)S(1)} %collective-permute-done.12), channel_id=1, source_target_pairs={{0,2},{2,0},{4,6},{6,4},{8,10},{10,8},{12,14},{14,12},{1,3},{3,1},... | collective-permute-start | bytes 884744 | tf_op jit(solution)/shard_map/ppermute | solution.py:28
  45.4 6.4 %collective-permute-start.14 = (bf16[144,1024]{1,0:T(8,128)(2,1)S(1)}, bf16[144,1024]{1,0:T(8,128)(2,1)S(1)}, u32[]{:S(2)}, u32[]{:S(2)}) collective-permute-start(bf16[144,1024]{1,0:T(8,128)(2,1)S(1)} %collective-permute-done.12), channel_id=1, source_target_pairs={{0,1},{1,0},{2,3},{3,2},{4,5},{5,4},{6,7},{7,6},{8,9},{9,8},{10,11... | collective-permute-start | bytes 884744 | tf_op jit(solution)/shard_map/ppermute | solution.py:25
  46.8 35.5 %collective-permute-start.3 = (bf16[288,1024]{1,0:T(8,128)(2,1)S(1)}, bf16[288,1024]{1,0:T(8,128)(2,1)S(1)}, u32[]{:S(2)}, u32[]{:S(2)}) collective-permute-start(bf16[288,1024]{1,0:T(8,128)(2,1)S(1)} %fusion.96), channel_id=1, source_target_pairs={{0,1},{1,0},{2,3},{3,2},{4,5},{5,4},{6,7},{7,6},{8,9},{9,8},{10,11... | collective-permute-start | bytes 1769480 | tf_op jit(solution)/shard_map/ppermute | solution.py:25
  47.7 8.0 %collective-permute-start.7 = (bf16[144,1024]{1,0:T(8,128)(2,1)S(1)}, bf16[144,1024]{1,0:T(8,128)(2,1)S(1)}, u32[]{:S(2)}, u32[]{:S(2)}) collective-permute-start(bf16[144,1024]{1,0:T(8,128)(2,1)S(1)} %collective-permute-done.5), channel_id=1, source_target_pairs={{0,1},{1,0},{2,3},{3,2},{4,5},{5,4},{6,7},{7,6},{8,9},{9,8},{10,11... | collective-permute-start | bytes 884744 | tf_op jit(solution)/shard_map/ppermute | solution.py:25
  49.1 7.4 %collective-permute-start.11 = (bf16[144,1024]{1,0:T(8,128)(2,1)S(1)}, bf16[144,1024]{1,0:T(8,128)(2,1)S(1)}, u32[]{:S(2)}, u32[]{:S(2)}) collective-permute-start(bf16[144,1024]{1,0:T(8,128)(2,1)S(1)} %collective-permute-done.9), channel_id=1, source_target_pairs={{0,1},{1,0},{2,3},{3,2},{4,5},{5,4},{6,7},{7,6},{8,9},{9,8},{10,11... | collective-permute-start | bytes 884744 | tf_op jit(solution)/shard_map/ppermute | solution.py:25
  59.8 20.2 %collective-permute-start.17 = (bf16[288,1024]{1,0:T(8,128)(2,1)S(1)}, bf16[288,1024]{1,0:T(8,128)(2,1)S(1)}, u32[]{:S(2)}, u32[]{:S(2)}) collective-permute-start(bf16[288,1024]{1,0:T(8,128)(2,1)S(1)} %fusion.102), channel_id=1, source_target_pairs={{0,1},{1,0},{2,3},{3,2},{4,5},{5,4},{6,7},{7,6},{8,9},{9,8},{10,11... | collective-permute-start | bytes 1769480 | tf_op jit(solution)/shard_map/ppermute | solution.py:25
  60.2 9.5 %collective-permute-start.20 = (bf16[144,1024]{1,0:T(8,128)(2,1)S(1)}, bf16[144,1024]{1,0:T(8,128)(2,1)S(1)}, u32[]{:S(2)}, u32[]{:S(2)}) collective-permute-start(bf16[144,1024]{1,0:T(8,128)(2,1)S(1)} %slice.45), channel_id=1, source_target_pairs={{0,2},{2,0},{4,6},{6,4},{8,10},{10,8},{12,14},{14,12},{1,3},{3,1},... | collective-permute-start | bytes 884744 | tf_op jit(solution)/shard_map/ppermute | solution.py:28
  69.7 16.3 %collective-permute-start.21 = (bf16[144,1024]{1,0:T(8,128)(2,1)S(1)}, bf16[144,1024]{1,0:T(8,128)(2,1)S(1)}, u32[]{:S(2)}, u32[]{:S(2)}) collective-permute-start(bf16[144,1024]{1,0:T(8,128)(2,1)S(1)} %add_convert_fusion.6), channel_id=1, source_target_pairs={{0,12},{2,14},{4,0},{6,2},{8,4},{10,6},{12,8},{14,10},{1,13},{3,15... | collective-permute-start | bytes 884744 | tf_op jit(solution)/shard_map/ppermute | solution.py:31
  81.6 9.7 %collective-permute-start.18 = (bf16[288,1024]{1,0:T(8,128)(2,1)S(1)}, bf16[288,1024]{1,0:T(8,128)(2,1)S(1)}, u32[]{:S(2)}, u32[]{:S(2)}) collective-permute-start(bf16[288,1024]{1,0:T(8,128)(2,1)S(1)} %fusion.105), channel_id=1, source_target_pairs={{0,1},{1,0},{2,3},{3,2},{4,5},{5,4},{6,7},{7,6},{8,9},{9,8},{10,11... | collective-permute-start | bytes 1769480 | tf_op jit(solution)/shard_map/ppermute | solution.py:25
  81.7 9.5 %collective-permute-start.22 = (bf16[144,1024]{1,0:T(8,128)(2,1)S(1)}, bf16[144,1024]{1,0:T(8,128)(2,1)S(1)}, u32[]{:S(2)}, u32[]{:S(2)}) collective-permute-start(bf16[144,1024]{1,0:T(8,128)(2,1)S(1)} %slice.47), channel_id=1, source_target_pairs={{0,2},{2,0},{4,6},{6,4},{8,10},{10,8},{12,14},{14,12},{1,3},{3,1},... | collective-permute-start | bytes 884744 | tf_op jit(solution)/shard_map/ppermute | solution.py:28
  91.2 10.4 %collective-permute-start.23 = (bf16[144,1024]{1,0:T(8,128)(2,1)S(1)}, bf16[144,1024]{1,0:T(8,128)(2,1)S(1)}, u32[]{:S(2)}, u32[]{:S(2)}) collective-permute-start(bf16[144,1024]{1,0:T(8,128)(2,1)S(1)} %add_convert_fusion.5), channel_id=1, source_target_pairs={{0,4},{2,6},{4,8},{6,10},{8,12},{10,14},{12,0},{14,2},{1,5},{3,7},... | collective-permute-start | bytes 884744 | tf_op jit(solution)/shard_map/ppermute | solution.py:31
  92.1 10.5 %collective-permute-start.24 = (bf16[144,1024]{1,0:T(8,128)(2,1)S(1)}, bf16[144,1024]{1,0:T(8,128)(2,1)S(1)}, u32[]{:S(2)}, u32[]{:S(2)}) collective-permute-start(bf16[144,1024]{1,0:T(8,128)(2,1)S(1)} %slice.97), channel_id=1, source_target_pairs={{0,2},{2,0},{4,6},{6,4},{8,10},{10,8},{12,14},{14,12},{1,3},{3,1},... | collective-permute-start | bytes 884744 | tf_op jit(solution)/shard_map/ppermute | solution.py:28
  102.0 7.8 %collective-permute-start.19 = (bf16[144,1024]{1,0:T(8,128)(2,1)S(1)}, bf16[144,1024]{1,0:T(8,128)(2,1)S(1)}, u32[]{:S(2)}, u32[]{:S(2)}) collective-permute-start(bf16[144,1024]{1,0:T(8,128)(2,1)S(1)} %slice.41), channel_id=1, source_target_pairs={{0,2},{2,0},{4,6},{6,4},{8,10},{10,8},{12,14},{14,12},{1,3},{3,1},... | collective-permute-start | bytes 884744 | tf_op jit(solution)/shard_map/ppermute | solution.py:28
  102.7 13.7 %collective-permute-start.25 = (bf16[144,1024]{1,0:T(8,128)(2,1)S(1)}, bf16[144,1024]{1,0:T(8,128)(2,1)S(1)}, u32[]{:S(2)}, u32[]{:S(2)}) collective-permute-start(bf16[144,1024]{1,0:T(8,128)(2,1)S(1)} %add_convert_fusion.4), channel_id=1, source_target_pairs={{0,8},{2,10},{4,12},{6,14},{8,0},{10,2},{12,4},{14,6},{1,9},{3,11}... | collective-permute-start | bytes 884744 | tf_op jit(solution)/shard_map/ppermute | solution.py:31
  (8 other events, 37.4 us)
where the time goes:
time: 121 us
  waiting for transfers between devices  54.1 us (45%)
  matrix products  26.1 us (22%)
  starting transfers between devices  26 us (21%)
  blocking collectives  5.09 us (4%)
  local copies, waits for them, and re-layouts  4.64 us (4%)
  other arithmetic  4.51 us (4%)
    ppermute x6, waiting for transfers between devices, shift_pair(): lax.ppermute(value, 'ep', [(i, (i + 2 * step) % ep_size) for i in range(e...  33.8 us
    ppermute x8, waiting for transfers between devices, swap_half(): return lax.ppermute(value, 'ep', [(i, i ^ 1) for i in range(ep_size)])  20.3 us
    ppermute x6, starting transfers between devices, shift_pair(): lax.ppermute(value, 'ep', [(i, (i + 2 * step) % ep_size) for i in range(e...  15.4 us
    ppermute x8, starting transfers between devices, swap_half(): return lax.ppermute(value, 'ep', [(i, i ^ 1) for i in range(ep_size)])  8.09 us
    dot_general x4, matrix products, shards(): jnp.dot(here, gate_own, preferred_element_type=f32)  4.77 us
    dot_general x4, matrix products, shards(): jnp.dot(there, up_other, preferred_element_type=f32)  3.43 us
    dot_general x4, matrix products, shards(): jnp.dot(hidden, down_own, preferred_element_type=f32).astype(bf16)  3.16 us
    dot_general x4, matrix products, shards(): jnp.dot(hidden, down_other, preferred_element_type=f32).astype(bf16)  3.15 us
  transfers between devices with their start and end apart: 26, of which 9 were waited for; matrix products, arithmetic and copies ran while one was open for 20% of the time, Pallas kernels for 0%

commit v1 on v0

--- a/solution.py
+++ b/solution.py
@@ -30,33 +30,33 @@
     def shift_pair(value, step):
         return lax.ppermute(value, "ep", [(i, (i + 2 * step) % ep_size) for i in range(ep_size)])
 
-    flat_ids = expert_ids.reshape(-1)
-    onehot = (flat_ids[:, None] == jnp.arange(expert_count, dtype=jnp.int32)[None, :]).astype(
-        jnp.int32
-    )
-    before = jnp.cumsum(onehot, axis=0) - onehot
-    slots = jnp.sum(before * onehot, axis=1).reshape(tok_rows, picks)
-    away = (expert_ids - pair + expert_count) % expert_count
-    targets = away * capacity + slots
-
     own_float = tokens.astype(f32)
-    squares = lax.psum(jnp.sum(own_float * own_float, axis=1), "tp")
-    factor = lax.rsqrt(squares / full_width + norm_eps)[:, None]
-    own_gain = lax.dynamic_slice_in_dim(gain_in, own_cols, half_width)
-    normed = (own_float * factor * own_gain).astype(bf16)
+    own_squares = jnp.sum(own_float * own_float, axis=1)
+    squares = own_squares + swap_core(own_squares)
 
     steps = [0]
     for near in range(1, expert_count // 2 + 1):
         steps += [near] if 2 * near == expert_count else [near, expert_count - near]
 
-    def pack(step):
-        rows = jnp.arange(capacity, dtype=jnp.int32)[:, None] + step * capacity
-        placing = jnp.zeros((capacity, tok_rows), bf16)
-        for which in range(picks):
-            placing = placing + (rows == targets[None, :, which]).astype(bf16)
+    experts = (pair + jnp.array(steps, jnp.int32)) % expert_count
+    named_by = expert_ids.T[None, :, :] == experts[:, None, None]
+    named = jnp.any(named_by, axis=1)
+    weights = jnp.sum(jnp.where(named_by, route_weight.T[None, :, :], 0.0), axis=1)
+    token = jnp.arange(tok_rows, dtype=jnp.int32)
+    earlier = (token[:, None] < token[None, :]).astype(bf16)
+    counts = jnp.dot(named.astype(bf16), earlier, preferred_element_type=f32)
+    slots = jnp.where(named, counts.astype(jnp.int32), -1)
+    slot_rows = jnp.arange(capacity, dtype=jnp.int32)[:, None]
+
+    factor = lax.rsqrt(squares / full_width + norm_eps)[:, None]
+    own_gain = lax.dynamic_slice_in_dim(gain_in, own_cols, half_width)
+    normed = (own_float * factor * own_gain).astype(bf16)
+
+    def pack(k):
+        placing = (slot_rows == slots[k][None, :]).astype(bf16)
         return jnp.dot(placing, normed, preferred_element_type=f32).astype(bf16)
 
-    sent = [pack(step) for step in steps]
+    sent = [pack(k) for k in range(expert_count)]
     mine = [sent[0]]
     for k, step in enumerate(steps[1:], 1):
         mine.append(shift_pair(sent[k], step))
@@ -96,19 +96,16 @@
         whole = (half_sums[k][:capacity].astype(f32) + crossed.astype(f32)).astype(bf16)
         returned.append(whole if step == 0 else shift_pair(whole, -step))
 
-    high = lax.reduce_precision(route_weight, 8, 7)
-    low = (route_weight - high).astype(bf16)
+    high = lax.reduce_precision(weights, 8, 7)
+    low = (weights - high).astype(bf16)
     high = high.astype(bf16)
     routed = jnp.zeros((tok_rows, half_width), f32)
-    for k, step in enumerate(steps):
-        cols = jnp.arange(capacity, dtype=jnp.int32)[None, :] + step * capacity
+    for k in range(expert_count):
         for weight in (high, low):
-            mixing = jnp.zeros((tok_rows, capacity), bf16)
-            for which in range(picks):
-                mixing = mixing + jnp.where(
-                    cols == targets[:, which][:, None], weight[:, which][:, None], jnp.zeros((), bf16)
-                )
-            routed = routed + jnp.dot(mixing, returned[k], preferred_element_type=f32)
+            mixing = jnp.where(slot_rows == slots[k][None, :], weight[k][None, :], jnp.zeros((), bf16))
+            routed = routed + lax.dot_general(
+                mixing, returned[k], (((0,), (0,)), ((), ())), preferred_element_type=f32
+            )
     squares_out = lax.psum(jnp.sum(routed * routed, axis=1), "tp")
     factor_out = lax.rsqrt(squares_out / full_width + norm_eps)[:, None]
     own_gain_out = lax.dynamic_slice_in_dim(gain_out, own_cols, half_width)

time: 121 us -> 119 us (0.983)
  blocking collectives: 5.09 us -> 2.47 us
  waiting for transfers between devices: 54.1 us -> 55.6 us
    psum x1 -> x0, blocking collectives: 2.62 us -> none  [shards(): squares = lax.psum(jnp.sum(own_float * own_float, axis=1), 'tp')]
    dot_general x4, matrix products: 4.77 us -> 3.11 us  [shards(): jnp.dot(here, gate_own, preferred_element_type=f32)]
    another operation x2 -> x0, other arithmetic: 1.41 us -> none
    ppermute x8, waiting for transfers between devices: 20.3 us -> 21.6 us  [swap_half(): return lax.ppermute(value, 'ep', [(i, i ^ 1) for i in range(ep_size)])]
    ppermute x12 -> x13, starting transfers between devices: 2.55 us -> 3.24 us  [swap_core(): return lax.ppermute(value, 'tp', [(0, 1), (1, 0)])]
    unnamed x18 -> x15, local copies, waits for them, and re-layouts: 2.95 us -> 2.57 us
    dot_general x8 -> x9, matrix products: 3.03 us -> 2.83 us  [the longest x8 2.69 us: shards(): lax.dot_general(mixing, returned[k], (((0,), (0,)), ((), ())), preferred_...]
  transfers between devices with their start and end apart: 26 -> 27, of which waited for: 9 -> 9; matrix products, arithmetic and copies ran while one was open for 20% -> 22% of each run, Pallas kernels for 0% -> 0%
where the time goes in v1:
time: 119 us; the launch traced here: 118 us
  waiting for transfers between devices  55.6 us (47%)
  starting transfers between devices  26.2 us (22%)
  matrix products  25.2 us (21%)
  other arithmetic  4.56 us (4%)
  local copies, waits for them, and re-layouts  3.54 us (3%)
  blocking collectives  2.47 us (2%)
    ppermute x6, waiting for transfers between devices, shift_pair(): lax.ppermute(value, 'ep', [(i, (i + 2 * step) % ep_size) for i in range(e...  34 us
    ppermute x8, waiting for transfers between devices, swap_half(): return lax.ppermute(value, 'ep', [(i, i ^ 1) for i in range(ep_size)])  21.6 us
    ppermute x6, starting transfers between devices, shift_pair(): lax.ppermute(value, 'ep', [(i, (i + 2 * step) % ep_size) for i in range(e...  15.4 us
    ppermute x8, starting transfers between devices, swap_half(): return lax.ppermute(value, 'ep', [(i, i ^ 1) for i in range(ep_size)])  7.64 us
    dot_general x4, matrix products, shards(): jnp.dot(there, up_other, preferred_element_type=f32)  3.43 us
    dot_general x4, matrix products, pack(): return jnp.dot(placing, normed, preferred_element_type=f32).astype(bf16)  3.37 us
    ppermute x13, starting transfers between devices, swap_core(): return lax.ppermute(value, 'tp', [(0, 1), (1, 0)])  3.24 us
    dot_general x4, matrix products, shards(): jnp.dot(there, gate_other, preferred_element_type=f32)  3.15 us
  transfers between devices with their start and end apart: 27, of which 9 were waited for; matrix products, arithmetic and copies ran while one was open for 22% of the time, Pallas kernels for 0%

profile of v1, /device:TPU:0, one launch (start us, length us, event | category | flops | bytes accessed | tf_op | source)
XLA Modules:
  0.0 118.2 jit_solution(5997074129284028140)
XLA Ops:
  0.0 1.2 %fusion.139 = f32[192]{0:T(256)S(1)} fusion(bf16[192,1024]{1,0:T(8,128)(2,1)} %param.9), kind=kLoop, calls=%fused_computation.115 | loop fusion | flops 589632 | bytes 393984 | tf_op jit(solution)/shard_map/reduce_sum | solution.py:34
  4.9 1.3 %convolution_convert_fusion.3 = bf16[144,1024]{1,0:T(8,128)(2,1)S(1)} fusion(s32[192]{0:T(256)S(1)} %bitcast.154, bf16[192,1024]{1,0:T(8,128)(2,1)} %param.9, f32[1024]{0:T(1024)S(1)} %dynamic_slice.36, f32[192]{0:T(256)S(1)} %add_rsqrt_fusion.1), kind=kOutput, calls=%fused_computation.78 | convolution fusion | flops 57584640 | bytes 693760 | tf_op jit(solution)/shard_map/dot_general | solution.py:57
  6.3 2.6 %collective-permute-start.1 = (bf16[144,1024]{1,0:T(8,128)(2,1)S(1)}, bf16[144,1024]{1,0:T(8,128)(2,1)S(1)}, u32[]{:S(2)}, u32[]{:S(2)}) collective-permute-start(bf16[144,1024]{1,0:T(8,128)(2,1)S(1)} %convolution_convert_fusion.3), channel_id=1, source_target_pairs={{0,2},{2,0},{4,6},{6,4},{8,10},{10,8},{12,14},{14,12},{1,3},{3,1},... | collective-permute-start | bytes 884744 | tf_op jit(solution)/shard_map/ppermute | solution.py:28
  9.1 1.3 %convolution_convert_fusion.2 = bf16[144,1024]{1,0:T(8,128)(2,1)S(1)} fusion(s32[192]{0:T(256)S(1)} %bitcast.145, bf16[192,1024]{1,0:T(8,128)(2,1)} %param.9, f32[1024]{0:T(1024)S(1)} %dynamic_slice.36, f32[192]{0:T(256)S(1)} %add_rsqrt_fusion.1), kind=kOutput, calls=%fused_computation.77 | convolution fusion | flops 57584640 | bytes 693760 | tf_op jit(solution)/shard_map/dot_general | solution.py:57
  10.4 2.7 %collective-permute-start.5 = (bf16[144,1024]{1,0:T(8,128)(2,1)S(1)}, bf16[144,1024]{1,0:T(8,128)(2,1)S(1)}, u32[]{:S(2)}, u32[]{:S(2)}) collective-permute-start(bf16[144,1024]{1,0:T(8,128)(2,1)S(1)} %convolution_convert_fusion.2), channel_id=1, source_target_pairs={{0,8},{2,10},{4,12},{6,14},{8,0},{10,2},{12,4},{14,6},{1,9},{3,11}... | collective-permute-start | bytes 884744 | tf_op jit(solution)/shard_map/ppermute | solution.py:31
  13.4 1.4 %collective-permute-start.9 = (bf16[144,1024]{1,0:T(8,128)(2,1)S(1)}, bf16[144,1024]{1,0:T(8,128)(2,1)S(1)}, u32[]{:S(2)}, u32[]{:S(2)}) collective-permute-start(bf16[144,1024]{1,0:T(8,128)(2,1)S(1)} %convolution_convert_fusion.1), channel_id=1, source_target_pairs={{0,12},{2,14},{4,0},{6,2},{8,4},{10,6},{12,8},{14,10},{1,13},{3,15... | collective-permute-start | bytes 884744 | tf_op jit(solution)/shard_map/ppermute | solution.py:31
  15.9 12.0 %collective-permute-done.5 = bf16[144,1024]{1,0:T(8,128)(2,1)S(1)} collective-permute-done((bf16[144,1024]{1,0:T(8,128)(2,1)S(1)}, bf16[144,1024]{1,0:T(8,128)(2,1)S(1)}, u32[]{:S(2)}, u32[]{:S(2)}) %collective-permute-start.5) | collective-permute-done | bytes 294944 | tf_op jit(solution)/shard_map/ppermute | solution.py:31
  28.2 1.9 %collective-permute-start.10 = (bf16[144,1024]{1,0:T(8,128)(2,1)S(1)}, bf16[144,1024]{1,0:T(8,128)(2,1)S(1)}, u32[]{:S(2)}, u32[]{:S(2)}) collective-permute-start(bf16[144,1024]{1,0:T(8,128)(2,1)S(1)} %collective-permute-done.9), channel_id=1, source_target_pairs={{0,2},{2,0},{4,6},{6,4},{8,10},{10,8},{12,14},{14,12},{1,3},{3,1},... | collective-permute-start | bytes 884744 | tf_op jit(solution)/shard_map/ppermute | solution.py:28
  30.5 3.9 %collective-permute-done.13 = bf16[144,1024]{1,0:T(8,128)(2,1)S(1)} collective-permute-done((bf16[144,1024]{1,0:T(8,128)(2,1)S(1)}, bf16[144,1024]{1,0:T(8,128)(2,1)S(1)}, u32[]{:S(2)}, u32[]{:S(2)}) %collective-permute-start.13) | collective-permute-done | bytes 294944 | tf_op jit(solution)/shard_map/ppermute | solution.py:31
  35.2 1.2 %copy-done.2 = bf16[1,2048,896]{2,1,0:T(8,128)(2,1)S(1)} copy-done((bf16[1,2048,896]{2,1,0:T(8,128)(2,1)S(1)}, bf16[1,2048,896]{2,1,0:T(8,128)(2,1)}, u32[]{:S(2)}) %copy-start.2) | copy-done | bytes 3670040
  38.7 0.9 multiply_convert_fusion.3
  39.5 1.2 copy-done.3
  46.0 2.0 %collective-permute-done.14 = bf16[144,1024]{1,0:T(8,128)(2,1)S(1)} collective-permute-done((bf16[144,1024]{1,0:T(8,128)(2,1)S(1)}, bf16[144,1024]{1,0:T(8,128)(2,1)S(1)}, u32[]{:S(2)}, u32[]{:S(2)}) %collective-permute-start.14) | collective-permute-done | bytes 294944 | tf_op jit(solution)/shard_map/ppermute | solution.py:28
  50.5 0.9 multiply_convert_fusion
  54.4 0.9 multiply_convert_fusion.1
  58.6 8.0 %collective-permute-done.21 = bf16[144,1024]{1,0:T(8,128)(2,1)S(1)} collective-permute-done((bf16[144,1024]{1,0:T(8,128)(2,1)S(1)}, bf16[144,1024]{1,0:T(8,128)(2,1)S(1)}, u32[]{:S(2)}, u32[]{:S(2)}) %collective-permute-start.21) | collective-permute-done | bytes 294944 | tf_op jit(solution)/shard_map/ppermute | solution.py:28
  66.7 10.5 %collective-permute-start.22 = (bf16[144,1024]{1,0:T(8,128)(2,1)S(1)}, bf16[144,1024]{1,0:T(8,128)(2,1)S(1)}, u32[]{:S(2)}, u32[]{:S(2)}) collective-permute-start(bf16[144,1024]{1,0:T(8,128)(2,1)S(1)} %add_convert_fusion.6), channel_id=1, source_target_pairs={{0,12},{2,14},{4,0},{6,2},{8,4},{10,6},{12,8},{14,10},{1,13},{3,15... | collective-permute-start | bytes 884744 | tf_op jit(solution)/shard_map/ppermute | solution.py:31
  80.2 3.0 %collective-permute-done.22 = bf16[144,1024]{1,0:T(8,128)(2,1)S(1)} collective-permute-done((bf16[144,1024]{1,0:T(8,128)(2,1)S(1)}, bf16[144,1024]{1,0:T(8,128)(2,1)S(1)}, u32[]{:S(2)}, u32[]{:S(2)}) %collective-permute-start.22) | collective-permute-done | bytes 294944 | tf_op jit(solution)/shard_map/ppermute | solution.py:31
  83.5 4.8 %collective-permute-done.23 = bf16[144,1024]{1,0:T(8,128)(2,1)S(1)} collective-permute-done((bf16[144,1024]{1,0:T(8,128)(2,1)S(1)}, bf16[144,1024]{1,0:T(8,128)(2,1)S(1)}, u32[]{:S(2)}, u32[]{:S(2)}) %collective-permute-start.23) | collective-permute-done | bytes 294944 | tf_op jit(solution)/shard_map/ppermute | solution.py:28
  90.2 8.6 %collective-permute-done.24 = bf16[144,1024]{1,0:T(8,128)(2,1)S(1)} collective-permute-done((bf16[144,1024]{1,0:T(8,128)(2,1)S(1)}, bf16[144,1024]{1,0:T(8,128)(2,1)S(1)}, u32[]{:S(2)}, u32[]{:S(2)}) %collective-permute-start.24) | collective-permute-done | bytes 294944 | tf_op jit(solution)/shard_map/ppermute | solution.py:31
  100.2 6.7 %collective-permute-done.20 = bf16[144,1024]{1,0:T(8,128)(2,1)S(1)} collective-permute-done((bf16[144,1024]{1,0:T(8,128)(2,1)S(1)}, bf16[144,1024]{1,0:T(8,128)(2,1)S(1)}, u32[]{:S(2)}, u32[]{:S(2)}) %collective-permute-start.20) | collective-permute-done | bytes 294944 | tf_op jit(solution)/shard_map/ppermute | solution.py:28
  107.2 6.4 %collective-permute-done.26 = bf16[144,1024]{1,0:T(8,128)(2,1)S(1)} collective-permute-done((bf16[144,1024]{1,0:T(8,128)(2,1)S(1)}, bf16[144,1024]{1,0:T(8,128)(2,1)S(1)}, u32[]{:S(2)}, u32[]{:S(2)}) %collective-permute-start.26) | collective-permute-done | bytes 294944 | tf_op jit(solution)/shard_map/ppermute | solution.py:31
  114.8 2.5 %psum.7 = f32[192]{0:T(256)S(1)} all-reduce(f32[192]{0:T(256)S(1)} %get-tuple-element.31), channel_id=1, replica_groups=mesh['grp'=2,'ep'=8,'tp'=2] {'tp'}, use_global_device_ids=true, to_apply=%region_4.5 | all-reduce | flops 192 | bytes 1536 | tf_op jit(solution)/shard_map/psum | solution.py:109
  117.3 0.9 multiply_convert_fusion.4
  (110 shorter events, 30.9 us)
Async XLA Ops:
  1.2 3.7 %collective-permute-start = (f32[192]{0:T(256)S(1)}, f32[192]{0:T(256)S(1)}, u32[]{:S(2)}, u32[]{:S(2)}) collective-permute-start(f32[192]{0:T(256)S(1)} %fusion.139), channel_id=1, source_target_pairs={{0,1},{1,0},{2,3},{3,2},{4,5},{5,4},{6,7},{7,6},{8,9},{9,8},{10,11... | collective-permute-start | bytes 2312 | tf_op jit(solution)/shard_map/ppermute | solution.py:25
  6.3 23.9 %collective-permute-start.1 = (bf16[144,1024]{1,0:T(8,128)(2,1)S(1)}, bf16[144,1024]{1,0:T(8,128)(2,1)S(1)}, u32[]{:S(2)}, u32[]{:S(2)}) collective-permute-start(bf16[144,1024]{1,0:T(8,128)(2,1)S(1)} %convolution_convert_fusion.3), channel_id=1, source_target_pairs={{0,2},{2,0},{4,6},{6,4},{8,10},{10,8},{12,14},{14,12},{1,3},{3,1},... | collective-permute-start | bytes 884744 | tf_op jit(solution)/shard_map/ppermute | solution.py:28
  8.9 19.4 %collective-permute-start.2 = (bf16[144,1024]{1,0:T(8,128)(2,1)S(1)}, bf16[144,1024]{1,0:T(8,128)(2,1)S(1)}, u32[]{:S(2)}, u32[]{:S(2)}) collective-permute-start(bf16[144,1024]{1,0:T(8,128)(2,1)S(1)} %convolution_convert_fusion.3), channel_id=1, source_target_pairs={{0,1},{1,0},{2,3},{3,2},{4,5},{5,4},{6,7},{7,6},{8,9},{9,8},{10,11... | collective-permute-start | bytes 884744 | tf_op jit(solution)/shard_map/ppermute | solution.py:25
  10.4 17.5 %collective-permute-start.5 = (bf16[144,1024]{1,0:T(8,128)(2,1)S(1)}, bf16[144,1024]{1,0:T(8,128)(2,1)S(1)}, u32[]{:S(2)}, u32[]{:S(2)}) collective-permute-start(bf16[144,1024]{1,0:T(8,128)(2,1)S(1)} %convolution_convert_fusion.2), channel_id=1, source_target_pairs={{0,8},{2,10},{4,12},{6,14},{8,0},{10,2},{12,4},{14,6},{1,9},{3,11}... | collective-permute-start | bytes 884744 | tf_op jit(solution)/shard_map/ppermute | solution.py:31
  13.4 14.8 %collective-permute-start.9 = (bf16[144,1024]{1,0:T(8,128)(2,1)S(1)}, bf16[144,1024]{1,0:T(8,128)(2,1)S(1)}, u32[]{:S(2)}, u32[]{:S(2)}) collective-permute-start(bf16[144,1024]{1,0:T(8,128)(2,1)S(1)} %convolution_convert_fusion.1), channel_id=1, source_target_pairs={{0,12},{2,14},{4,0},{6,2},{8,4},{10,6},{12,8},{14,10},{1,13},{3,15... | collective-permute-start | bytes 884744 | tf_op jit(solution)/shard_map/ppermute | solution.py:31
  15.1 19.2 %collective-permute-start.13 = (bf16[144,1024]{1,0:T(8,128)(2,1)S(1)}, bf16[144,1024]{1,0:T(8,128)(2,1)S(1)}, u32[]{:S(2)}, u32[]{:S(2)}) collective-permute-start(bf16[144,1024]{1,0:T(8,128)(2,1)S(1)} %convolution_convert_fusion), channel_id=1, source_target_pairs={{0,4},{2,6},{4,8},{6,10},{8,12},{10,14},{12,0},{14,2},{1,5},{3,7},... | collective-permute-start | bytes 884744 | tf_op jit(solution)/shard_map/ppermute | solution.py:31
  27.9 13.6 %collective-permute-start.6 = (bf16[144,1024]{1,0:T(8,128)(2,1)S(1)}, bf16[144,1024]{1,0:T(8,128)(2,1)S(1)}, u32[]{:S(2)}, u32[]{:S(2)}) collective-permute-start(bf16[144,1024]{1,0:T(8,128)(2,1)S(1)} %collective-permute-done.5), channel_id=1, source_target_pairs={{0,2},{2,0},{4,6},{6,4},{8,10},{10,8},{12,14},{14,12},{1,3},{3,1},... | collective-permute-start | bytes 884744 | tf_op jit(solution)/shard_map/ppermute | solution.py:28
  28.2 14.4 %collective-permute-start.7 = (bf16[144,1024]{1,0:T(8,128)(2,1)S(1)}, bf16[144,1024]{1,0:T(8,128)(2,1)S(1)}, u32[]{:S(2)}, u32[]{:S(2)}) collective-permute-start(bf16[144,1024]{1,0:T(8,128)(2,1)S(1)} %collective-permute-done.5), channel_id=1, source_target_pairs={{0,1},{1,0},{2,3},{3,2},{4,5},{5,4},{6,7},{7,6},{8,9},{9,8},{10,11... | collective-permute-start | bytes 884744 | tf_op jit(solution)/shard_map/ppermute | solution.py:25
  28.2 15.5 %collective-permute-start.10 = (bf16[144,1024]{1,0:T(8,128)(2,1)S(1)}, bf16[144,1024]{1,0:T(8,128)(2,1)S(1)}, u32[]{:S(2)}, u32[]{:S(2)}) collective-permute-start(bf16[144,1024]{1,0:T(8,128)(2,1)S(1)} %collective-permute-done.9), channel_id=1, source_target_pairs={{0,2},{2,0},{4,6},{6,4},{8,10},{10,8},{12,14},{14,12},{1,3},{3,1},... | collective-permute-start | bytes 884744 | tf_op jit(solution)/shard_map/ppermute | solution.py:28
  30.2 14.7 %collective-permute-start.11 = (bf16[144,1024]{1,0:T(8,128)(2,1)S(1)}, bf16[144,1024]{1,0:T(8,128)(2,1)S(1)}, u32[]{:S(2)}, u32[]{:S(2)}) collective-permute-start(bf16[144,1024]{1,0:T(8,128)(2,1)S(1)} %collective-permute-done.9), channel_id=1, source_target_pairs={{0,1},{1,0},{2,3},{3,2},{4,5},{5,4},{6,7},{7,6},{8,9},{9,8},{10,11... | collective-permute-start | bytes 884744 | tf_op jit(solution)/shard_map/ppermute | solution.py:25
  37.3 10.8 %collective-permute-start.14 = (bf16[144,1024]{1,0:T(8,128)(2,1)S(1)}, bf16[144,1024]{1,0:T(8,128)(2,1)S(1)}, u32[]{:S(2)}, u32[]{:S(2)}) collective-permute-start(bf16[144,1024]{1,0:T(8,128)(2,1)S(1)} %collective-permute-done.13), channel_id=1, source_target_pairs={{0,2},{2,0},{4,6},{6,4},{8,10},{10,8},{12,14},{14,12},{1,3},{3,1},... | collective-permute-start | bytes 884744 | tf_op jit(solution)/shard_map/ppermute | solution.py:28
  41.5 7.4 %collective-permute-start.15 = (bf16[144,1024]{1,0:T(8,128)(2,1)S(1)}, bf16[144,1024]{1,0:T(8,128)(2,1)S(1)}, u32[]{:S(2)}, u32[]{:S(2)}) collective-permute-start(bf16[144,1024]{1,0:T(8,128)(2,1)S(1)} %collective-permute-done.13), channel_id=1, source_target_pairs={{0,1},{1,0},{2,3},{3,2},{4,5},{5,4},{6,7},{7,6},{8,9},{9,8},{10,11... | collective-permute-start | bytes 884744 | tf_op jit(solution)/shard_map/ppermute | solution.py:25
  42.6 36.8 %collective-permute-start.4 = (bf16[288,1024]{1,0:T(8,128)(2,1)S(1)}, bf16[288,1024]{1,0:T(8,128)(2,1)S(1)}, u32[]{:S(2)}, u32[]{:S(2)}) collective-permute-start(bf16[288,1024]{1,0:T(8,128)(2,1)S(1)} %fusion.96), channel_id=1, source_target_pairs={{0,1},{1,0},{2,3},{3,2},{4,5},{5,4},{6,7},{7,6},{8,9},{9,8},{10,11... | collective-permute-start | bytes 1769480 | tf_op jit(solution)/shard_map/ppermute | solution.py:25
  43.8 9.0 %collective-permute-start.8 = (bf16[144,1024]{1,0:T(8,128)(2,1)S(1)}, bf16[144,1024]{1,0:T(8,128)(2,1)S(1)}, u32[]{:S(2)}, u32[]{:S(2)}) collective-permute-start(bf16[144,1024]{1,0:T(8,128)(2,1)S(1)} %collective-permute-done.6), channel_id=1, source_target_pairs={{0,1},{1,0},{2,3},{3,2},{4,5},{5,4},{6,7},{7,6},{8,9},{9,8},{10,11... | collective-permute-start | bytes 884744 | tf_op jit(solution)/shard_map/ppermute | solution.py:25
  44.9 8.7 %collective-permute-start.12 = (bf16[144,1024]{1,0:T(8,128)(2,1)S(1)}, bf16[144,1024]{1,0:T(8,128)(2,1)S(1)}, u32[]{:S(2)}, u32[]{:S(2)}) collective-permute-start(bf16[144,1024]{1,0:T(8,128)(2,1)S(1)} %collective-permute-done.10), channel_id=1, source_target_pairs={{0,1},{1,0},{2,3},{3,2},{4,5},{5,4},{6,7},{7,6},{8,9},{9,8},{10,11... | collective-permute-start | bytes 884744 | tf_op jit(solution)/shard_map/ppermute | solution.py:25
  56.9 20.3 %collective-permute-start.18 = (bf16[288,1024]{1,0:T(8,128)(2,1)S(1)}, bf16[288,1024]{1,0:T(8,128)(2,1)S(1)}, u32[]{:S(2)}, u32[]{:S(2)}) collective-permute-start(bf16[288,1024]{1,0:T(8,128)(2,1)S(1)} %fusion.102), channel_id=1, source_target_pairs={{0,1},{1,0},{2,3},{3,2},{4,5},{5,4},{6,7},{7,6},{8,9},{9,8},{10,11... | collective-permute-start | bytes 1769480 | tf_op jit(solution)/shard_map/ppermute | solution.py:25
  57.2 9.5 %collective-permute-start.21 = (bf16[144,1024]{1,0:T(8,128)(2,1)S(1)}, bf16[144,1024]{1,0:T(8,128)(2,1)S(1)}, u32[]{:S(2)}, u32[]{:S(2)}) collective-permute-start(bf16[144,1024]{1,0:T(8,128)(2,1)S(1)} %slice.78), channel_id=1, source_target_pairs={{0,2},{2,0},{4,6},{6,4},{8,10},{10,8},{12,14},{14,12},{1,3},{3,1},... | collective-permute-start | bytes 884744 | tf_op jit(solution)/shard_map/ppermute | solution.py:28
  66.7 16.5 %collective-permute-start.22 = (bf16[144,1024]{1,0:T(8,128)(2,1)S(1)}, bf16[144,1024]{1,0:T(8,128)(2,1)S(1)}, u32[]{:S(2)}, u32[]{:S(2)}) collective-permute-start(bf16[144,1024]{1,0:T(8,128)(2,1)S(1)} %add_convert_fusion.6), channel_id=1, source_target_pairs={{0,12},{2,14},{4,0},{6,2},{8,4},{10,6},{12,8},{14,10},{1,13},{3,15... | collective-permute-start | bytes 884744 | tf_op jit(solution)/shard_map/ppermute | solution.py:31
  78.7 9.7 %collective-permute-start.19 = (bf16[288,1024]{1,0:T(8,128)(2,1)S(1)}, bf16[288,1024]{1,0:T(8,128)(2,1)S(1)}, u32[]{:S(2)}, u32[]{:S(2)}) collective-permute-start(bf16[288,1024]{1,0:T(8,128)(2,1)S(1)} %fusion.105), channel_id=1, source_target_pairs={{0,1},{1,0},{2,3},{3,2},{4,5},{5,4},{6,7},{7,6},{8,9},{9,8},{10,11... | collective-permute-start | bytes 1769480 | tf_op jit(solution)/shard_map/ppermute | solution.py:25
  78.9 9.5 %collective-permute-start.23 = (bf16[144,1024]{1,0:T(8,128)(2,1)S(1)}, bf16[144,1024]{1,0:T(8,128)(2,1)S(1)}, u32[]{:S(2)}, u32[]{:S(2)}) collective-permute-start(bf16[144,1024]{1,0:T(8,128)(2,1)S(1)} %slice.82), channel_id=1, source_target_pairs={{0,2},{2,0},{4,6},{6,4},{8,10},{10,8},{12,14},{14,12},{1,3},{3,1},... | collective-permute-start | bytes 884744 | tf_op jit(solution)/shard_map/ppermute | solution.py:28
  88.4 10.4 %collective-permute-start.24 = (bf16[144,1024]{1,0:T(8,128)(2,1)S(1)}, bf16[144,1024]{1,0:T(8,128)(2,1)S(1)}, u32[]{:S(2)}, u32[]{:S(2)}) collective-permute-start(bf16[144,1024]{1,0:T(8,128)(2,1)S(1)} %add_convert_fusion.5), channel_id=1, source_target_pairs={{0,4},{2,6},{4,8},{6,10},{8,12},{10,14},{12,0},{14,2},{1,5},{3,7},... | collective-permute-start | bytes 884744 | tf_op jit(solution)/shard_map/ppermute | solution.py:31
  89.3 10.4 %collective-permute-start.25 = (bf16[144,1024]{1,0:T(8,128)(2,1)S(1)}, bf16[144,1024]{1,0:T(8,128)(2,1)S(1)}, u32[]{:S(2)}, u32[]{:S(2)}) collective-permute-start(bf16[144,1024]{1,0:T(8,128)(2,1)S(1)} %slice.86), channel_id=1, source_target_pairs={{0,2},{2,0},{4,6},{6,4},{8,10},{10,8},{12,14},{14,12},{1,3},{3,1},... | collective-permute-start | bytes 884744 | tf_op jit(solution)/shard_map/ppermute | solution.py:28
  99.1 7.8 %collective-permute-start.20 = (bf16[144,1024]{1,0:T(8,128)(2,1)S(1)}, bf16[144,1024]{1,0:T(8,128)(2,1)S(1)}, u32[]{:S(2)}, u32[]{:S(2)}) collective-permute-start(bf16[144,1024]{1,0:T(8,128)(2,1)S(1)} %slice.74), channel_id=1, source_target_pairs={{0,2},{2,0},{4,6},{6,4},{8,10},{10,8},{12,14},{14,12},{1,3},{3,1},... | collective-permute-start | bytes 884744 | tf_op jit(solution)/shard_map/ppermute | solution.py:28
  99.8 13.8 %collective-permute-start.26 = (bf16[144,1024]{1,0:T(8,128)(2,1)S(1)}, bf16[144,1024]{1,0:T(8,128)(2,1)S(1)}, u32[]{:S(2)}, u32[]{:S(2)}) collective-permute-start(bf16[144,1024]{1,0:T(8,128)(2,1)S(1)} %add_convert_fusion.4), channel_id=1, source_target_pairs={{0,8},{2,10},{4,12},{6,14},{8,0},{10,2},{12,4},{14,6},{1,9},{3,11}... | collective-permute-start | bytes 884744 | tf_op jit(solution)/shard_map/ppermute | solution.py:31
  (8 other events, 49.2 us)
